TPU v7x, 256 devices: a whole 4x4x8 slice. The times are simulated.
256 devices in a mesh: ep: 16 (over y, x), tp: 16 (over z, core).
Axes of the slice: x: 4, y: 4, z: 8, core: 2. Of those that a mesh axis runs over, the one named last changes fastest.
Arguments:
- hidden_in: bfloat16 [256, 4096], P('ep'), may hold values from -6 to 6
- attn_gain: float32 [4096], replicated, may hold values from 0.1 to 1.9
- query_weight: bfloat16 [4096, 4096], P('ep', 'tp'), may hold values from -0.09375 to 0.09375
- key_weight: bfloat16 [4096, 2048], P('ep', 'tp'), may hold values from -0.09375 to 0.09375
- value_weight: bfloat16 [4096, 2048], P('ep', 'tp'), may hold values from -0.09375 to 0.09375
- query_gain: float32 [128], replicated, may hold values from 0.1 to 1.9
- key_gain: float32 [128], replicated, may hold values from 0.1 to 1.9
- head_offset: float32 [32], P('tp'), may hold values from -7 to -2
- key_cache: bfloat16 [256, 1024, 2048], P('ep', None, 'tp'), may hold values from -6 to 6
- value_cache: bfloat16 [256, 1024, 2048], P('ep', None, 'tp'), may hold values from -6 to 6
- lengths: int32 [256], P('ep'), may hold values from 1 to 1024
- out_weight: bfloat16 [4096, 4096], P('tp', 'ep'), may hold values from -0.375 to 0.375
- expert_gain: float32 [4096], replicated, may hold values from 0.1 to 1.9
- routes: int32 [256, 2], P('ep'), may hold values from 0 to 15, all different within a row; in each aligned block of 16 rows (0 to 15, 16 to 31, ...) at most 4 rows name the same one
- route_weights: float32 [256, 2], P('ep'), may hold values from 0.1 to 1
- gate_weight: bfloat16 [16, 4096, 2048], P('ep', None, 'tp'), may hold values from -0.09375 to 0.09375
- up_weight: bfloat16 [16, 4096, 2048], P('ep', None, 'tp'), may hold values from -0.09375 to 0.09375
- down_weight: bfloat16 [16, 2048, 4096], P('ep', 'tp'), may hold values from -0.125 to 0.125
Outputs:
- layer_out: bfloat16 [256, 4096], P('ep', 'tp')
- fresh_keys: bfloat16 [256, 2048], P('ep', 'tp')
- fresh_values: bfloat16 [256, 2048], P('ep', 'tp')
Inputs may be any that keep to these rules, and one draw needn't show every extreme that they name: `routes`: each row names 2 different experts. Among the rows of one index of ep (16 rows) no expert is named more than 4 times, a bound that some block reaches.
All inputs are finite; a program needn't handle non-finite values.
Results may differ from a plain program's by a relative error of at most 0.018.
Values may be sent and summed in bfloat16 or wider, within the bound.
A program may use at most 64 MiB of HBM per device.

v0:
```python
import jax
import jax.numpy as jnp
from jax import lax
from jax.sharding import PartitionSpec as P

EPSILON = 1e-06


def split_up(shard, dim, size):
    shape = shard.shape
    tiles = shard.reshape(*shape[:dim], size, shape[dim] // size, *shape[dim + 1 :])
    return jnp.moveaxis(tiles, dim, 0)


def sent_and_summed(shard, axis, dim):
    size = lax.axis_size(axis)
    tiles = lax.all_to_all(split_up(shard, dim, size), axis, 0, 0, tiled=True)
    return jnp.sum(tiles.astype(jnp.float32), axis=0)


def joined_along(tiles, dim):
    tiles = jnp.moveaxis(tiles, 0, dim)
    shape = tiles.shape
    return tiles.reshape(*shape[:dim], shape[dim] * shape[dim + 1], *shape[dim + 2 :])


def sent_to_all(shard, axis):
    size = lax.axis_size(axis)
    return lax.all_to_all(
        jnp.broadcast_to(shard[None], (size, *shard.shape)), axis, 0, 0, tiled=True
    )


def gather_directly(shard, axis, dim):
    return joined_along(sent_to_all(shard, axis), dim)


def over_copies(shard, axis):
    return sent_to_all(shard, axis).sum(axis=0)


def norm_rows(values, gain):
    meansq = jnp.mean(values * values, axis=-1, keepdims=True)
    return values * lax.rsqrt(meansq + EPSILON) * gain


def body(
    hidden_in,
    attn_gain,
    query_weight,
    key_weight,
    value_weight,
    query_gain,
    key_gain,
    head_offset,
    key_cache,
    value_cache,
    lengths,
    out_weight,
    expert_gain,
    routes,
    route_weights,
    gate_weight,
    up_weight,
    down_weight,
):
    count_ep = lax.axis_size("ep")
    count_tp = lax.axis_size("tp")
    seqs_here = hidden_in.shape[0]
    width = hidden_in.shape[1]
    head_dim = query_gain.shape[0]
    query_cols = query_weight.shape[1]
    pair_cols = key_weight.shape[1]
    kv_here = pair_cols // head_dim
    groups = query_cols // pair_cols
    cache_len = key_cache.shape[1]
    x_float = hidden_in.astype(jnp.float32)
    normed = norm_rows(x_float, attn_gain).astype(jnp.bfloat16)
    slices = lax.all_to_all(normed, "ep", split_axis=1, concat_axis=0, tiled=True)
    summed = sent_and_summed(
        jnp.concatenate(
            [
                jnp.dot(slices, query_weight, preferred_element_type=jnp.float32),
                jnp.dot(slices, key_weight, preferred_element_type=jnp.float32),
                jnp.dot(slices, value_weight, preferred_element_type=jnp.float32),
            ],
            axis=1,
        ).astype(jnp.bfloat16),
        "ep",
        0,
    )
    query_raw = summed[:, :query_cols].astype(jnp.bfloat16)
    key_raw = summed[:, query_cols : query_cols + pair_cols].astype(jnp.bfloat16)
    fresh_values = summed[:, query_cols + pair_cols :].astype(jnp.bfloat16)
    query = norm_rows(
        query_raw.astype(jnp.float32).reshape(seqs_here, query_cols // head_dim, head_dim),
        query_gain,
    ).astype(jnp.bfloat16)
    fresh_keys = norm_rows(
        key_raw.astype(jnp.float32).reshape(seqs_here, kv_here, head_dim), key_gain
    ).astype(jnp.bfloat16)
    grouped = query.reshape(seqs_here, kv_here, groups, head_dim)
    cached_keys = key_cache.reshape(seqs_here, cache_len, kv_here, head_dim)
    cached_values = value_cache.reshape(seqs_here, cache_len, kv_here, head_dim)
    scores = jnp.einsum("bkgd,bskd->bkgs", grouped, cached_keys, preferred_element_type=jnp.float32)
    scores = scores * head_dim ** (-0.5) + head_offset.reshape(kv_here, groups)[None, :, :, None]
    positions = lax.broadcasted_iota(jnp.int32, (1, 1, 1, cache_len), 3)
    live = positions < lengths[:, None, None, None]
    breaks = jnp.where(live, jax.nn.softplus(scores), 0.0)
    suffix = lax.cumsum(breaks, axis=3, reverse=True) - breaks
    stick = jnp.where(live, jnp.exp(jax.nn.log_sigmoid(scores) - suffix), 0.0).astype(jnp.bfloat16)
    attended = jnp.einsum(
        "bkgs,bskd->bkgd", stick, cached_values, preferred_element_type=jnp.float32
    )
    attended = attended.astype(jnp.bfloat16).reshape(seqs_here, query_cols)
    terms = jnp.dot(
        gather_directly(attended, "ep", 0), out_weight, preferred_element_type=jnp.float32
    )
    partial_value = lax.all_to_all(
        terms.astype(jnp.bfloat16), "ep", split_axis=0, concat_axis=1, tiled=True
    ).astype(terms.dtype)
    top = routes.shape[1]
    capacity = seqs_here * top * 2 // count_ep
    slots_all = count_ep * capacity
    flat = routes.reshape(-1)
    onehot = (flat[:, None] == lax.broadcasted_iota(jnp.int32, (1, count_ep), 1)).astype(jnp.int32)
    before = jnp.cumsum(onehot, axis=0) - onehot
    rank = jnp.sum(before * onehot, axis=1)
    slot = flat * capacity + rank
    match = (slot[:, None] == lax.broadcasted_iota(jnp.int32, (1, slots_all), 1)).astype(
        jnp.float32
    )
    match = match.reshape(seqs_here, top, slots_all)
    dispatch = jnp.sum(match, axis=1).astype(jnp.bfloat16)
    combine = jnp.sum(match * route_weights[:, :, None], axis=1)
    share_width = width // count_tp
    col_start = lax.axis_index("tp") * share_width
    projected_share = sent_and_summed(partial_value.astype(jnp.bfloat16), "tp", 1)
    own_share = lax.dynamic_slice_in_dim(x_float, col_start, share_width, 1)
    residual_share = (own_share + projected_share).astype(jnp.bfloat16)
    share_float = residual_share.astype(jnp.float32)
    squares = over_copies(jnp.sum(share_float * share_float, axis=1), "tp")
    gain_share = lax.dynamic_slice_in_dim(expert_gain, col_start, share_width, 0)
    expert_share = (
        share_float * lax.rsqrt(squares / width + EPSILON)[:, None] * gain_share
    ).astype(jnp.bfloat16)
    outgoing = jnp.einsum(
        "sj,sd->jd", dispatch, expert_share, preferred_element_type=jnp.float32
    ).astype(jnp.bfloat16)
    moved = lax.all_to_all(outgoing, "ep", split_axis=0, concat_axis=0, tiled=True)
    arrived = lax.all_gather(moved, "tp", axis=1, tiled=True)
    gate = jnp.dot(arrived, gate_weight[0], preferred_element_type=jnp.float32)
    upward = jnp.dot(arrived, up_weight[0], preferred_element_type=jnp.float32)
    hidden = (jax.nn.silu(gate) * upward).astype(jnp.bfloat16)
    expert_terms = jnp.dot(hidden, down_weight[0], preferred_element_type=jnp.float32)
    expert_out = sent_and_summed(expert_terms.astype(jnp.bfloat16), "tp", 1).astype(jnp.bfloat16)
    returned = lax.all_to_all(expert_out, "ep", split_axis=0, concat_axis=0, tiled=True)
    mixed = jnp.dot(combine, returned.astype(jnp.float32), precision=lax.Precision.HIGHEST)
    layer_out = (residual_share.astype(jnp.float32) + mixed).astype(jnp.bfloat16)
    return (layer_out, fresh_keys.reshape(seqs_here, pair_cols), fresh_values)


def solution(mesh):
    placed = (
        P("ep", None),
        P(),
        P("ep", "tp"),
        P("ep", "tp"),
        P("ep", "tp"),
        P(),
        P(),
        P("tp"),
        P("ep", None, "tp"),
        P("ep", None, "tp"),
        P("ep"),
        P("tp", "ep"),
        P(),
        P("ep", None),
        P("ep", None),
        P("ep", None, "tp"),
        P("ep", None, "tp"),
        P("ep", "tp", None),
    )
    return jax.shard_map(
        body,
        mesh=mesh,
        in_specs=placed,
        out_specs=(P("ep", "tp"), P("ep", "tp"), P("ep", "tp")),
        check_vma=False,
    )
```

profile of v0, /device:TPU:1, one launch (start us, length us, event | category | flops | bytes accessed | tf_op | source)
XLA Modules:
  0.0 199.3 jit_solution(7542754235354447465)
XLA Ops:
  0.6 1.1 multiply_reduce_fusion
  1.8 1.0 multiply_convert_fusion
  2.8 14.2 %all_to_all.79 = bf16[16,16,256]{2,0,1:T(8,128)(2,1)S(1)} all-to-all(bf16[16,16,256]{2,0,1:T(8,128)(2,1)S(1)} %bitcast.66), channel_id=1, replica_groups=mesh['ep'=16,'tp'=16] {'ep'}, dimensions={1} | all-to-all | bytes 262144 | tf_op jit(solution)/shard_map/all_to_all | solution.py:79
  17.1 1.0 convolution_convert_fusion.4
  18.1 1.0 convolution_convert_fusion.3
  19.1 1.1 convolution_convert_fusion.2
  20.2 0.7 pad_maximum_fusion
  20.9 3.5 %all-to-all-start.1 = ((bf16[16,16,512]{2,1,0:T(8,128)(2,1)}), bf16[16,16,512]{2,1,0:T(8,128)(2,1)S(1)}, u32[]{:S(2)}, u32[]{:S(2)}) async-start(bf16[16,16,512]{2,1,0:T(8,128)(2,1)} %pad_maximum_fusion), calls=%async_computation.1 | async-start | bytes 524288 | tf_op jit(solution)/shard_map/all_to_all | solution.py:17
  24.5 0.7 iota_compare_fusion
  25.2 6.8 %all-to-all-done.1 = bf16[16,16,512]{2,1,0:T(8,128)(2,1)S(1)} async-done(((bf16[16,16,512]{2,1,0:T(8,128)(2,1)}), bf16[16,16,512]{2,1,0:T(8,128)(2,1)S(1)}, u32[]{:S(2)}, u32[]{:S(2)}) %all-to-all-start.1) | async-done | bytes 262176 | tf_op jit(solution)/shard_map/all_to_all | solution.py:17
  32.2 3.4 %fusion.11 = (f32[16,2,1024]{2,1,0:T(2,128)S(1)}, f32[16,2,1024]{2,1,0:T(2,128)S(1)}) fusion(pred[16,1024]{1,0:T(8,128)(4,1)S(1)} %iota_compare_fusion, f32[2]{0:T(128)} %param.25, bf16[16,1024,128]{2,1,0:T(8,128)(2,1)} %param.26, f32[16,2,128]{2,1,0:T(2,128)S(1)} %reshape.212, f32[128]{0:T(128)} %param.23, f32[16,2]{1,0:T(8,128)S(1)} %add_rsqrt_fusion), kind=kOutput, calls=%fused_computation.27 | convolution fusion | flops 8695808 | bytes 4489864 | tf_op jit(solution)/shard_map/bkgd,bskd->bkgs/dot_general | solution.py:105
  35.8 39.6 %reduce-window.6 = f32[16,1,2,8,128]{4,3,2,1,0:T(8,128)S(1)} reduce-window(f32[16,1,2,8,128]{4,3,2,1,0:T(8,128)S(1)} %bitcast.67, f32[]{:T(128)} %constant.22.clone.1), window={size=1x1x1x1x128 pad=0_0x0_0x0_0x0_0x0_127}, to_apply=%region_3.0 | reduce-window | flops 4161536 | bytes 262148 | tf_op jit(solution)/shard_map/reduce-window
  76.0 3.4 %convolution_convert_fusion.6 = bf16[16,2,128]{2,1,0:T(2,128)(2,1)S(1)} fusion(bf16[16,1024,128]{2,1,0:T(8,128)(2,1)} %param.27, pred[16,1024]{1,0:T(8,128)(4,1)S(1)} %iota_compare_fusion, f32[16,2,1024]{2,1,0:T(2,128)S(1)} %reshape.205, f32[16,2,1024]{2,1,0:T(2,128)S(1)} %reshape.208, f32[16,2,1024]{2,1,0:T(2,128)S(1)} %get-tuple-element.8), kind=kOutput, calls=%fused_computation.12 | convolution fusion | flops 9048064 | bytes 4612096 | tf_op jit(solution)/shard_map/bkgs,bskd->bkgd/dot_general | solution.py:112
  80.0 3.5 %all-to-all-start.2 = ((bf16[16,16,256]{2,1,0:T(8,128)(2,1)}), bf16[16,16,256]{2,1,0:T(8,128)(2,1)S(1)}, u32[]{:S(2)}, u32[]{:S(2)}) async-start(bf16[16,16,256]{2,1,0:T(8,128)(2,1)} %broadcast_in_dim.22), calls=%async_computation.2 | async-start | bytes 262144 | tf_op jit(solution)/shard_map/all_to_all | solution.py:29
  83.7 6.6 %all-to-all-done.2 = bf16[16,16,256]{2,1,0:T(8,128)(2,1)S(1)} async-done(((bf16[16,16,256]{2,1,0:T(8,128)(2,1)}), bf16[16,16,256]{2,1,0:T(8,128)(2,1)S(1)}, u32[]{:S(2)}, u32[]{:S(2)}) %all-to-all-start.2) | async-done | bytes 131104 | tf_op jit(solution)/shard_map/all_to_all | solution.py:29
  90.3 0.8 convolution_convert_fusion.1
  91.2 4.2 %all-to-all-start.3 = ((bf16[16,16,256]{2,1,0:T(8,128)(2,1)}), bf16[16,16,256]{2,1,0:T(8,128)(2,1)}, u32[]{:S(2)}, u32[]{:S(2)}) async-start(bf16[16,16,256]{2,1,0:T(8,128)(2,1)} %bitcast.8), calls=%async_computation.3 | async-start | bytes 262144 | tf_op jit(solution)/shard_map/all_to_all | solution.py:119
  95.5 6.7 %all-to-all-done.3 = bf16[16,16,256]{2,1,0:T(8,128)(2,1)} async-done(((bf16[16,16,256]{2,1,0:T(8,128)(2,1)}), bf16[16,16,256]{2,1,0:T(8,128)(2,1)}, u32[]{:S(2)}, u32[]{:S(2)}) %all-to-all-start.3) | async-done | bytes 131104 | tf_op jit(solution)/shard_map/all_to_all | solution.py:119
  102.2 14.0 %all-to-all-start.4 = ((bf16[16,16,256]{2,1,0:T(8,128)(2,1)}), bf16[16,16,256]{2,1,0:T(8,128)(2,1)S(1)}, u32[]{:S(2)}, u32[]{:S(2)}) async-start(bf16[16,16,256]{2,1,0:T(8,128)(2,1)} %all-to-all-done.3), calls=%async_computation.4 | async-start | bytes 262144 | tf_op jit(solution)/shard_map/all_to_all | solution.py:17
  116.6 8.5 %all-to-all-done.4 = bf16[16,16,256]{2,1,0:T(8,128)(2,1)S(1)} async-done(((bf16[16,16,256]{2,1,0:T(8,128)(2,1)}), bf16[16,16,256]{2,1,0:T(8,128)(2,1)S(1)}, u32[]{:S(2)}, u32[]{:S(2)}) %all-to-all-start.4) | async-done | bytes 131104 | tf_op jit(solution)/shard_map/all_to_all | solution.py:17
  125.8 3.4 %all-to-all-start.5 = ((f32[16,1,16]{2,1,0:T(1,128)}), f32[16,1,16]{2,1,0:T(1,128)S(1)}, u32[]{:S(2)}, u32[]{:S(2)}) async-start(f32[16,1,16]{2,1,0:T(1,128)} %broadcast_in_dim.23), calls=%async_computation.5 | async-start | bytes 16384 | tf_op jit(solution)/shard_map/all_to_all | solution.py:29
  129.3 0.8 dynamic_slice.7
  130.1 5.9 %all-to-all-done.5 = f32[16,1,16]{2,1,0:T(1,128)S(1)} async-done(((f32[16,1,16]{2,1,0:T(1,128)}), f32[16,1,16]{2,1,0:T(1,128)S(1)}, u32[]{:S(2)}, u32[]{:S(2)}) %all-to-all-start.5) | async-done | bytes 1056 | tf_op jit(solution)/shard_map/all_to_all | solution.py:29
  136.2 9.3 %all_to_all.80 = bf16[16,4,256]{2,1,0:T(4,128)(2,1)S(1)} all-to-all(bf16[16,4,256]{2,1,0:T(4,128)(2,1)S(1)} %all_to_all.63), channel_id=1, replica_groups=mesh['ep'=16,'tp'=16] {'ep'}, dimensions={0} | all-to-all | bytes 65536 | tf_op jit(solution)/shard_map/all_to_all | solution.py:150
  145.5 18.0 %all_gather.3 = bf16[64,4096]{1,0:T(8,128)(2,1)S(1)} all-gather(bf16[64,256]{1,0:T(8,128)(2,1)S(1)} %all_to_all.65), channel_id=1, replica_groups=mesh['ep'=16,'tp'=16] {'tp'}, dimensions={1}, use_global_device_ids=true | all-gather | bytes 557056 | tf_op jit(solution)/shard_map/all_gather | solution.py:151
  163.5 1.5 fusion.6
  165.7 0.8 copy.76
  166.6 4.2 %all-to-all-start.7 = ((bf16[16,64,256]{2,1,0:T(8,128)(2,1)}), bf16[16,64,256]{2,1,0:T(8,128)(2,1)S(1)}, u32[]{:S(2)}, u32[]{:S(2)}) async-start(bf16[16,64,256]{2,1,0:T(8,128)(2,1)} %bitcast.58), calls=%async_computation.7 | async-start | bytes 1048576 | tf_op jit(solution)/shard_map/all_to_all | solution.py:17
  170.9 17.1 %all-to-all-done.7 = bf16[16,64,256]{2,1,0:T(8,128)(2,1)S(1)} async-done(((bf16[16,64,256]{2,1,0:T(8,128)(2,1)}), bf16[16,64,256]{2,1,0:T(8,128)(2,1)S(1)}, u32[]{:S(2)}, u32[]{:S(2)}) %all-to-all-start.7) | async-done | bytes 524320 | tf_op jit(solution)/shard_map/all_to_all | solution.py:17
  188.6 3.5 %all-to-all-start.8 = ((bf16[16,4,256]{2,1,0:T(4,128)(2,1)}), bf16[16,4,256]{2,1,0:T(4,128)(2,1)S(1)}, u32[]{:S(2)}, u32[]{:S(2)}) async-start(bf16[16,4,256]{2,1,0:T(4,128)(2,1)} %all_to_all.67), calls=%async_computation.8 | async-start | bytes 65536 | tf_op jit(solution)/shard_map/all_to_all | solution.py:157
  193.4 5.1 %all-to-all-done.8 = bf16[16,4,256]{2,1,0:T(4,128)(2,1)S(1)} async-done(((bf16[16,4,256]{2,1,0:T(4,128)(2,1)}), bf16[16,4,256]{2,1,0:T(4,128)(2,1)S(1)}, u32[]{:S(2)}, u32[]{:S(2)}) %all-to-all-start.8) | async-done | bytes 32800 | tf_op jit(solution)/shard_map/all_to_all | solution.py:157
  198.6 0.7 fusion.2
  (57 shorter events, 6.0 us)
Async XLA Ops:
  0.6 164.5 %copy-start = (bf16[1,128,4096]{2,1,0:T(8,128)(2,1)S(1)}, bf16[1,128,4096]{2,1,0:T(8,128)(2,1)}, u32[]{:S(2)}) copy-start(bf16[1,128,4096]{2,1,0:T(8,128)(2,1)} %param.35) | copy-start | bytes 3145732
  20.9 11.0 %all-to-all-start.1 = ((bf16[16,16,512]{2,1,0:T(8,128)(2,1)}), bf16[16,16,512]{2,1,0:T(8,128)(2,1)S(1)}, u32[]{:S(2)}, u32[]{:S(2)}) async-start(bf16[16,16,512]{2,1,0:T(8,128)(2,1)} %pad_maximum_fusion), calls=%async_computation.1 | async-start | bytes 524288 | tf_op jit(solution)/shard_map/all_to_all | solution.py:17
  35.6 47.9 %copy-start.4 = (s32[16,2]{0,1:T(2,128)S(1)}, s32[16,2]{0,1:T(2,128)}, u32[]{:S(2)}) copy-start(s32[16,2]{0,1:T(2,128)} %param.31) | copy-start | bytes 388
  35.6 54.7 %copy-start.3 = (bf16[256,256]{1,0:T(8,128)(2,1)S(1)}, bf16[256,256]{1,0:T(8,128)(2,1)}, u32[]{:S(2)}) copy-start(bf16[256,256]{1,0:T(8,128)(2,1)} %param.29) | copy-start | bytes 393220
  35.8 80.6 %copy-start.1 = (bf16[16,4096]{1,0:T(8,128)(2,1)S(1)}, bf16[16,4096]{1,0:T(8,128)(2,1)}, u32[]{:S(2)}) copy-start(bf16[16,4096]{1,0:T(8,128)(2,1)} %param.18) | copy-start | bytes 393220
  75.5 53.7 %copy-start.5 = (f32[16,2]{0,1:T(2,128)S(1)}, f32[16,2]{0,1:T(2,128)}, u32[]{:S(2)}) copy-start(f32[16,2]{0,1:T(2,128)} %param.32) | copy-start | bytes 388
  76.0 89.1 %copy-start.2 = (bf16[1,4096,128]{2,1,0:T(8,128)(2,1)S(1)}, bf16[1,4096,128]{2,1,0:T(8,128)(2,1)}, u32[]{:S(2)}) copy-start(bf16[1,4096,128]{2,1,0:T(8,128)(2,1)} %param.34) | copy-start | bytes 3145732
  80.0 10.3 %all-to-all-start.2 = ((bf16[16,16,256]{2,1,0:T(8,128)(2,1)}), bf16[16,16,256]{2,1,0:T(8,128)(2,1)S(1)}, u32[]{:S(2)}, u32[]{:S(2)}) async-start(bf16[16,16,256]{2,1,0:T(8,128)(2,1)} %broadcast_in_dim.22), calls=%async_computation.2 | async-start | bytes 262144 | tf_op jit(solution)/shard_map/all_to_all | solution.py:29
  91.2 11.0 %all-to-all-start.3 = ((bf16[16,16,256]{2,1,0:T(8,128)(2,1)}), bf16[16,16,256]{2,1,0:T(8,128)(2,1)}, u32[]{:S(2)}, u32[]{:S(2)}) async-start(bf16[16,16,256]{2,1,0:T(8,128)(2,1)} %bitcast.8), calls=%async_computation.3 | async-start | bytes 262144 | tf_op jit(solution)/shard_map/all_to_all | solution.py:119
  102.2 22.9 %all-to-all-start.4 = ((bf16[16,16,256]{2,1,0:T(8,128)(2,1)}), bf16[16,16,256]{2,1,0:T(8,128)(2,1)S(1)}, u32[]{:S(2)}, u32[]{:S(2)}) async-start(bf16[16,16,256]{2,1,0:T(8,128)(2,1)} %all-to-all-done.3), calls=%async_computation.4 | async-start | bytes 262144 | tf_op jit(solution)/shard_map/all_to_all | solution.py:17
  125.8 10.1 %all-to-all-start.5 = ((f32[16,1,16]{2,1,0:T(1,128)}), f32[16,1,16]{2,1,0:T(1,128)S(1)}, u32[]{:S(2)}, u32[]{:S(2)}) async-start(f32[16,1,16]{2,1,0:T(1,128)} %broadcast_in_dim.23), calls=%async_computation.5 | async-start | bytes 16384 | tf_op jit(solution)/shard_map/all_to_all | solution.py:29
  136.0 56.2 %copy-start.6 = (f32[128]{0:T(128)S(1)}, f32[128]{0:T(128)}, u32[]{:S(2)}) copy-start(f32[128]{0:T(128)} %param.24) | copy-start | bytes 1540
  166.6 21.4 %all-to-all-start.7 = ((bf16[16,64,256]{2,1,0:T(8,128)(2,1)}), bf16[16,64,256]{2,1,0:T(8,128)(2,1)S(1)}, u32[]{:S(2)}, u32[]{:S(2)}) async-start(bf16[16,64,256]{2,1,0:T(8,128)(2,1)} %bitcast.58), calls=%async_computation.7 | async-start | bytes 1048576 | tf_op jit(solution)/shard_map/all_to_all | solution.py:17
  188.6 9.9 %all-to-all-start.8 = ((bf16[16,4,256]{2,1,0:T(4,128)(2,1)}), bf16[16,4,256]{2,1,0:T(4,128)(2,1)S(1)}, u32[]{:S(2)}, u32[]{:S(2)}) async-start(bf16[16,4,256]{2,1,0:T(4,128)(2,1)} %all_to_all.67), calls=%async_computation.8 | async-start | bytes 65536 | tf_op jit(solution)/shard_map/all_to_all | solution.py:157
where the time goes:
time: 200 us; the launch traced here: 199 us
  waiting for transfers between devices  56.7 us (28%)
  other arithmetic  44.9 us (22%)
  blocking collectives  41.5 us (21%)
  starting transfers between devices  36.3 us (18%)
  matrix products  13.8 us (7%)
  local copies, waits for them, and re-layouts  5.17 us (3%)
    another operation x2, other arithmetic  39.7 us
    all_to_all x3, waiting for transfers between devices, sent_and_summed(): tiles = lax.all_to_all(split_up(shard, dim, size), axis, 0, 0, tiled=True)  32.3 us
    all_to_all x3, starting transfers between devices, sent_and_summed(): tiles = lax.all_to_all(split_up(shard, dim, size), axis, 0, 0, tiled=True)  21.7 us
    all_gather x1, blocking collectives, body(): arrived = lax.all_gather(moved, 'tp', axis=1, tiled=True)  18 us
    all_to_all x1, blocking collectives, body(): lax.all_to_all(normed, 'ep', split_axis=1, concat_axis=0, tiled=True)  14.2 us
    all_to_all x2, waiting for transfers between devices, sent_to_all(): lax.all_to_all(jnp.broadcast_to(shard[None], (size, *shard.shape)), axis,...  12.5 us
    all_to_all x1, blocking collectives, body(): lax.all_to_all(outgoing, 'ep', split_axis=0, concat_axis=0, tiled=True)  9.26 us
    all_to_all x2, starting transfers between devices, sent_to_all(): lax.all_to_all(jnp.broadcast_to(shard[None], (size, *shard.shape)), axis,...  6.88 us
  transfers between devices with their start and end apart: 7, of which 7 were waited for; matrix products, arithmetic and copies ran while one was open for 2% of the time, Pallas kernels for 0%

commit v1 on v0

--- a/solution.py
+++ b/solution.py
@@ -148,7 +148,16 @@
         "sj,sd->jd", dispatch, expert_share, preferred_element_type=jnp.float32
     ).astype(jnp.bfloat16)
     moved = lax.all_to_all(outgoing, "ep", split_axis=0, concat_axis=0, tiled=True)
-    arrived = lax.all_gather(moved, "tp", axis=1, tiled=True)
+    ways = lax.axis_size("tp")
+    up = [(d, (d + 1) % ways) for d in range(ways)]
+    down = [(d, (d - 1) % ways) for d in range(ways)]
+    earlier, later = ([moved], [moved])
+    for _ in range(ways // 2):
+        earlier.append(lax.ppermute(earlier[-1], "tp", up))
+    for _ in range((ways - 1) // 2):
+        later.append(lax.ppermute(later[-1], "tp", down))
+    line = jnp.concatenate([*earlier[::-1], *later[1:]], axis=1)
+    arrived = jnp.roll(line, (lax.axis_index("tp") - ways // 2) * moved.shape[1], axis=1)
     gate = jnp.dot(arrived, gate_weight[0], preferred_element_type=jnp.float32)
     upward = jnp.dot(arrived, up_weight[0], preferred_element_type=jnp.float32)
     hidden = (jax.nn.silu(gate) * upward).astype(jnp.bfloat16)

time: 200 us -> 225 us (1.12)
  starting transfers between devices: 36.3 us -> 66.9 us
  blocking collectives: 41.5 us -> 23.5 us
  waiting for transfers between devices: 56.7 us -> 63 us
  local copies, waits for them, and re-layouts: 5.17 us -> 10.3 us
    ppermute x0 -> x15, starting transfers between devices: none -> 27.7 us  [the longest x7 21.1 us: body(): later.append(lax.ppermute(later[-1], 'tp', down))]
    all_gather x1 -> x0, blocking collectives: 18 us -> none  [body(): arrived = lax.all_gather(moved, 'tp', axis=1, tiled=True)]
    ppermute x0 -> x15, waiting for transfers between devices: none -> 6.65 us  [the longest x8 5.39 us: body(): earlier.append(lax.ppermute(earlier[-1], 'tp', up))]
    unnamed x16 -> x57, local copies, waits for them, and re-layouts: 0.14 us -> 5.27 us
    all_to_all x3, starting transfers between devices: 21.7 us -> 24.7 us  [sent_and_summed(): tiles = lax.all_to_all(split_up(shard, dim, size), axis, 0, 0, tiled=True)]
  transfers between devices with their start and end apart: 7 -> 22, of which waited for: 7 -> 19; matrix products, arithmetic and copies ran while one was open for 2% -> 3% of each run, Pallas kernels for 0% -> 0%
where the time goes in v1:
time: 225 us; the launch traced here: 224 us
  starting transfers between devices  66.9 us (30%)
  waiting for transfers between devices  63 us (28%)
  other arithmetic  45.5 us (20%)
  blocking collectives  23.5 us (10%)
  matrix products  13.8 us (6%)
  local copies, waits for them, and re-layouts  10.3 us (5%)
    another operation x2, other arithmetic  39.7 us
    all_to_all x3, waiting for transfers between devices, sent_and_summed(): tiles = lax.all_to_all(split_up(shard, dim, size), axis, 0, 0, tiled=True)  32.4 us
    all_to_all x3, starting transfers between devices, sent_and_summed(): tiles = lax.all_to_all(split_up(shard, dim, size), axis, 0, 0, tiled=True)  24.7 us
    ppermute x7, starting transfers between devices, body(): later.append(lax.ppermute(later[-1], 'tp', down))  21.1 us
    all_to_all x1, blocking collectives, body(): lax.all_to_all(normed, 'ep', split_axis=1, concat_axis=0, tiled=True)  14.2 us
    all_to_all x2, waiting for transfers between devices, sent_to_all(): lax.all_to_all(jnp.broadcast_to(shard[None], (size, *shard.shape)), axis,...  12.1 us
    all_to_all x1, blocking collectives, body(): lax.all_to_all(outgoing, 'ep', split_axis=0, concat_axis=0, tiled=True)  9.26 us
    all_to_all x2, starting transfers between devices, sent_to_all(): lax.all_to_all(jnp.broadcast_to(shard[None], (size, *shard.shape)), axis,...  6.84 us
  transfers between devices with their start and end apart: 22, of which 19 were waited for; matrix products, arithmetic and copies ran while one was open for 3% of the time, Pallas kernels for 0%

profile of v1, /device:TPU:1, one launch (start us, length us, event | category | flops | bytes accessed | tf_op | source)
XLA Modules:
  0.0 224.1 jit_solution(4876654007091405034)
XLA Ops:
  0.6 1.1 multiply_reduce_fusion
  2.8 14.2 %all_to_all.79 = bf16[16,16,256]{2,0,1:T(8,128)(2,1)S(1)} all-to-all(bf16[16,16,256]{2,0,1:T(8,128)(2,1)S(1)} %bitcast.67), channel_id=1, replica_groups=mesh['ep'=16,'tp'=16] {'ep'}, dimensions={1} | all-to-all | bytes 262144 | tf_op jit(solution)/shard_map/all_to_all | solution.py:79
  19.1 1.1 convolution_convert_fusion.2
  20.9 3.5 %all-to-all-start.1 = ((bf16[16,16,512]{2,1,0:T(8,128)(2,1)}), bf16[16,16,512]{2,1,0:T(8,128)(2,1)S(1)}, u32[]{:S(2)}, u32[]{:S(2)}) async-start(bf16[16,16,512]{2,1,0:T(8,128)(2,1)} %pad_maximum_fusion), calls=%async_computation.1 | async-start | bytes 524288 | tf_op jit(solution)/shard_map/all_to_all | solution.py:17
  25.2 6.8 %all-to-all-done.1 = bf16[16,16,512]{2,1,0:T(8,128)(2,1)S(1)} async-done(((bf16[16,16,512]{2,1,0:T(8,128)(2,1)}), bf16[16,16,512]{2,1,0:T(8,128)(2,1)S(1)}, u32[]{:S(2)}, u32[]{:S(2)}) %all-to-all-start.1) | async-done | bytes 262176 | tf_op jit(solution)/shard_map/all_to_all | solution.py:17
  32.2 3.4 %fusion.12 = (f32[16,2,1024]{2,1,0:T(2,128)S(1)}, f32[16,2,1024]{2,1,0:T(2,128)S(1)}) fusion(pred[16,1024]{1,0:T(8,128)(4,1)S(1)} %iota_compare_fusion, f32[2]{0:T(128)} %param.25, bf16[16,1024,128]{2,1,0:T(8,128)(2,1)} %param.26, f32[16,2,128]{2,1,0:T(2,128)S(1)} %reshape.212, f32[128]{0:T(128)} %param.23, f32[16,2]{1,0:T(8,128)S(1)} %add_rsqrt_fusion), kind=kOutput, calls=%fused_computation.28 | convolution fusion | flops 8695808 | bytes 4489864 | tf_op jit(solution)/shard_map/bkgd,bskd->bkgs/dot_general | solution.py:105
  35.8 39.6 %reduce-window.6 = f32[16,1,2,8,128]{4,3,2,1,0:T(8,128)S(1)} reduce-window(f32[16,1,2,8,128]{4,3,2,1,0:T(8,128)S(1)} %bitcast.68, f32[]{:T(128)} %constant.59.clone.1), window={size=1x1x1x1x128 pad=0_0x0_0x0_0x0_0x0_127}, to_apply=%region_3.0 | reduce-window | flops 4161536 | bytes 262148 | tf_op jit(solution)/shard_map/reduce-window
  76.0 3.3 %convolution_convert_fusion.6 = bf16[16,2,128]{2,1,0:T(2,128)(2,1)S(1)} fusion(bf16[16,1024,128]{2,1,0:T(8,128)(2,1)} %param.27, pred[16,1024]{1,0:T(8,128)(4,1)S(1)} %iota_compare_fusion, f32[16,2,1024]{2,1,0:T(2,128)S(1)} %reshape.205, f32[16,2,1024]{2,1,0:T(2,128)S(1)} %reshape.208, f32[16,2,1024]{2,1,0:T(2,128)S(1)} %get-tuple-element.8), kind=kOutput, calls=%fused_computation.10 | convolution fusion | flops 9048064 | bytes 4612096 | tf_op jit(solution)/shard_map/bkgs,bskd->bkgd/dot_general | solution.py:112
  79.9 3.5 %all-to-all-start.2 = ((bf16[16,16,256]{2,1,0:T(8,128)(2,1)}), bf16[16,16,256]{2,1,0:T(8,128)(2,1)S(1)}, u32[]{:S(2)}, u32[]{:S(2)}) async-start(bf16[16,16,256]{2,1,0:T(8,128)(2,1)} %broadcast_in_dim.22), calls=%async_computation.2 | async-start | bytes 262144 | tf_op jit(solution)/shard_map/all_to_all | solution.py:29
  83.6 6.6 %all-to-all-done.2 = bf16[16,16,256]{2,1,0:T(8,128)(2,1)S(1)} async-done(((bf16[16,16,256]{2,1,0:T(8,128)(2,1)}), bf16[16,16,256]{2,1,0:T(8,128)(2,1)S(1)}, u32[]{:S(2)}, u32[]{:S(2)}) %all-to-all-start.2) | async-done | bytes 131104 | tf_op jit(solution)/shard_map/all_to_all | solution.py:29
  91.1 4.2 %all-to-all-start.3 = ((bf16[16,16,256]{2,1,0:T(8,128)(2,1)}), bf16[16,16,256]{2,1,0:T(8,128)(2,1)}, u32[]{:S(2)}, u32[]{:S(2)}) async-start(bf16[16,16,256]{2,1,0:T(8,128)(2,1)} %bitcast.8), calls=%async_computation.3 | async-start | bytes 262144 | tf_op jit(solution)/shard_map/all_to_all | solution.py:119
  95.4 6.7 %all-to-all-done.3 = bf16[16,16,256]{2,1,0:T(8,128)(2,1)} async-done(((bf16[16,16,256]{2,1,0:T(8,128)(2,1)}), bf16[16,16,256]{2,1,0:T(8,128)(2,1)}, u32[]{:S(2)}, u32[]{:S(2)}) %all-to-all-start.3) | async-done | bytes 131104 | tf_op jit(solution)/shard_map/all_to_all | solution.py:119
  102.1 14.0 %all-to-all-start.4 = ((bf16[16,16,256]{2,1,0:T(8,128)(2,1)}), bf16[16,16,256]{2,1,0:T(8,128)(2,1)S(1)}, u32[]{:S(2)}, u32[]{:S(2)}) async-start(bf16[16,16,256]{2,1,0:T(8,128)(2,1)} %all-to-all-done.3), calls=%async_computation.4 | async-start | bytes 262144 | tf_op jit(solution)/shard_map/all_to_all | solution.py:17
  116.5 8.5 %all-to-all-done.4 = bf16[16,16,256]{2,1,0:T(8,128)(2,1)S(1)} async-done(((bf16[16,16,256]{2,1,0:T(8,128)(2,1)}), bf16[16,16,256]{2,1,0:T(8,128)(2,1)S(1)}, u32[]{:S(2)}, u32[]{:S(2)}) %all-to-all-start.4) | async-done | bytes 131104 | tf_op jit(solution)/shard_map/all_to_all | solution.py:17
  125.8 3.3 %all-to-all-start.5 = ((f32[16,1,16]{2,1,0:T(1,128)}), f32[16,1,16]{2,1,0:T(1,128)S(1)}, u32[]{:S(2)}, u32[]{:S(2)}) async-start(f32[16,1,16]{2,1,0:T(1,128)} %broadcast_in_dim.23), calls=%async_computation.5 | async-start | bytes 16384 | tf_op jit(solution)/shard_map/all_to_all | solution.py:29
  130.6 5.4 %all-to-all-done.5 = f32[16,1,16]{2,1,0:T(1,128)S(1)} async-done(((f32[16,1,16]{2,1,0:T(1,128)}), f32[16,1,16]{2,1,0:T(1,128)S(1)}, u32[]{:S(2)}, u32[]{:S(2)}) %all-to-all-start.5) | async-done | bytes 1056 | tf_op jit(solution)/shard_map/all_to_all | solution.py:29
  136.3 9.3 %all_to_all.80 = bf16[16,4,256]{2,1,0:T(4,128)(2,1)S(1)} all-to-all(bf16[16,4,256]{2,1,0:T(4,128)(2,1)S(1)} %all_to_all.63), channel_id=1, replica_groups=mesh['ep'=16,'tp'=16] {'ep'}, dimensions={0} | all-to-all | bytes 65536 | tf_op jit(solution)/shard_map/all_to_all | solution.py:150
  145.5 2.3 %collective-permute-start = (bf16[64,256]{1,0:T(8,128)(2,1)S(1)}, bf16[64,256]{1,0:T(8,128)(2,1)S(1)}, u32[]{:S(2)}, u32[]{:S(2)}) collective-permute-start(bf16[64,256]{1,0:T(8,128)(2,1)S(1)} %all_to_all.65), channel_id=1, source_target_pairs={{0,1},{1,2},{2,3},{3,4},{4,5},{5,6},{6,7},{7,8},{8,9},{9,10},{10,1... | collective-permute-start | bytes 98312 | tf_op jit(solution)/shard_map/ppermute | solution.py:156
  148.8 2.3 %collective-permute-start.1 = (bf16[64,256]{1,0:T(8,128)(2,1)S(1)}, bf16[64,256]{1,0:T(8,128)(2,1)S(1)}, u32[]{:S(2)}, u32[]{:S(2)}) collective-permute-start(bf16[64,256]{1,0:T(8,128)(2,1)S(1)} %collective-permute-done), channel_id=1, source_target_pairs={{0,1},{1,2},{2,3},{3,4},{4,5},{5,6},{6,7},{7,8},{8,9},{9,10},{10,1... | collective-permute-start | bytes 98312 | tf_op jit(solution)/shard_map/ppermute | solution.py:156
  151.1 1.1 collective-permute-start.8
  152.9 1.6 collective-permute-start.2
  154.5 2.3 %collective-permute-start.9 = (bf16[64,256]{1,0:T(8,128)(2,1)S(1)}, bf16[64,256]{1,0:T(8,128)(2,1)S(1)}, u32[]{:S(2)}, u32[]{:S(2)}) collective-permute-start(bf16[64,256]{1,0:T(8,128)(2,1)S(1)} %collective-permute-done.8), channel_id=1, source_target_pairs={{0,15},{1,0},{2,1},{3,2},{4,3},{5,4},{6,5},{7,6},{8,7},{9,8},{10,9... | collective-permute-start | bytes 98312 | tf_op jit(solution)/shard_map/ppermute | solution.py:158
  157.8 3.5 %collective-permute-start.10 = (bf16[64,256]{1,0:T(8,128)(2,1)S(1)}, bf16[64,256]{1,0:T(8,128)(2,1)S(1)}, u32[]{:S(2)}, u32[]{:S(2)}) collective-permute-start(bf16[64,256]{1,0:T(8,128)(2,1)S(1)} %collective-permute-done.9), channel_id=1, source_target_pairs={{0,15},{1,0},{2,1},{3,2},{4,3},{5,4},{6,5},{7,6},{8,7},{9,8},{10,9... | collective-permute-start | bytes 98312 | tf_op jit(solution)/shard_map/ppermute | solution.py:158
  162.2 3.7 %collective-permute-start.11 = (bf16[64,256]{1,0:T(8,128)(2,1)S(1)}, bf16[64,256]{1,0:T(8,128)(2,1)S(1)}, u32[]{:S(2)}, u32[]{:S(2)}) collective-permute-start(bf16[64,256]{1,0:T(8,128)(2,1)S(1)} %collective-permute-done.10), channel_id=1, source_target_pairs={{0,15},{1,0},{2,1},{3,2},{4,3},{5,4},{6,5},{7,6},{8,7},{9,8},{10,9... | collective-permute-start | bytes 98312 | tf_op jit(solution)/shard_map/ppermute | solution.py:158
  166.7 3.7 %collective-permute-start.12 = (bf16[64,256]{1,0:T(8,128)(2,1)S(1)}, bf16[64,256]{1,0:T(8,128)(2,1)S(1)}, u32[]{:S(2)}, u32[]{:S(2)}) collective-permute-start(bf16[64,256]{1,0:T(8,128)(2,1)S(1)} %collective-permute-done.11), channel_id=1, source_target_pairs={{0,15},{1,0},{2,1},{3,2},{4,3},{5,4},{6,5},{7,6},{8,7},{9,8},{10,9... | collective-permute-start | bytes 98312 | tf_op jit(solution)/shard_map/ppermute | solution.py:158
  171.7 3.8 %collective-permute-start.13 = (bf16[64,256]{1,0:T(8,128)(2,1)S(1)}, bf16[64,256]{1,0:T(8,128)(2,1)S(1)}, u32[]{:S(2)}, u32[]{:S(2)}) collective-permute-start(bf16[64,256]{1,0:T(8,128)(2,1)S(1)} %collective-permute-done.12), channel_id=1, source_target_pairs={{0,15},{1,0},{2,1},{3,2},{4,3},{5,4},{6,5},{7,6},{8,7},{9,8},{10,9... | collective-permute-start | bytes 98312 | tf_op jit(solution)/shard_map/ppermute | solution.py:158
  176.4 3.1 %collective-permute-start.14 = (bf16[64,256]{1,0:T(8,128)(2,1)S(1)}, bf16[64,256]{1,0:T(8,128)(2,1)S(1)}, u32[]{:S(2)}, u32[]{:S(2)}) collective-permute-start(bf16[64,256]{1,0:T(8,128)(2,1)S(1)} %collective-permute-done.13), channel_id=1, source_target_pairs={{0,15},{1,0},{2,1},{3,2},{4,3},{5,4},{6,5},{7,6},{8,7},{9,8},{10,9... | collective-permute-start | bytes 98312 | tf_op jit(solution)/shard_map/ppermute | solution.py:158
  185.6 1.8 convolution_convert_fusion
  188.3 7.2 %all-to-all-start.7 = ((bf16[16,64,256]{2,1,0:T(8,128)(2,1)}), bf16[16,64,256]{2,1,0:T(8,128)(2,1)S(1)}, u32[]{:S(2)}, u32[]{:S(2)}) async-start(bf16[16,64,256]{2,1,0:T(8,128)(2,1)} %bitcast.59), calls=%async_computation.7 | async-start | bytes 1048576 | tf_op jit(solution)/shard_map/all_to_all | solution.py:17
  195.5 17.2 %all-to-all-done.7 = bf16[16,64,256]{2,1,0:T(8,128)(2,1)S(1)} async-done(((bf16[16,64,256]{2,1,0:T(8,128)(2,1)}), bf16[16,64,256]{2,1,0:T(8,128)(2,1)S(1)}, u32[]{:S(2)}, u32[]{:S(2)}) %all-to-all-start.7) | async-done | bytes 524320 | tf_op jit(solution)/shard_map/all_to_all | solution.py:17
  213.4 3.5 %all-to-all-start.8 = ((bf16[16,4,256]{2,1,0:T(4,128)(2,1)}), bf16[16,4,256]{2,1,0:T(4,128)(2,1)S(1)}, u32[]{:S(2)}, u32[]{:S(2)}) async-start(bf16[16,4,256]{2,1,0:T(4,128)(2,1)} %all_to_all.67), calls=%async_computation.8 | async-start | bytes 65536 | tf_op jit(solution)/shard_map/all_to_all | solution.py:166
  218.2 5.1 %all-to-all-done.8 = bf16[16,4,256]{2,1,0:T(4,128)(2,1)S(1)} async-done(((bf16[16,4,256]{2,1,0:T(4,128)(2,1)}), bf16[16,4,256]{2,1,0:T(4,128)(2,1)S(1)}, u32[]{:S(2)}, u32[]{:S(2)}) %all-to-all-start.8) | async-done | bytes 32800 | tf_op jit(solution)/shard_map/all_to_all | solution.py:166
  (128 shorter events, 26.2 us)
Async XLA Ops:
  0.6 184.9 %copy-start = (bf16[1,128,4096]{2,1,0:T(8,128)(2,1)S(1)}, bf16[1,128,4096]{2,1,0:T(8,128)(2,1)}, u32[]{:S(2)}) copy-start(bf16[1,128,4096]{2,1,0:T(8,128)(2,1)} %param.35) | copy-start | bytes 3145732
  20.9 11.0 %all-to-all-start.1 = ((bf16[16,16,512]{2,1,0:T(8,128)(2,1)}), bf16[16,16,512]{2,1,0:T(8,128)(2,1)S(1)}, u32[]{:S(2)}, u32[]{:S(2)}) async-start(bf16[16,16,512]{2,1,0:T(8,128)(2,1)} %pad_maximum_fusion), calls=%async_computation.1 | async-start | bytes 524288 | tf_op jit(solution)/shard_map/all_to_all | solution.py:17
  35.6 47.9 %copy-start.9 = (s32[16,2]{0,1:T(2,128)S(1)}, s32[16,2]{0,1:T(2,128)}, u32[]{:S(2)}) copy-start(s32[16,2]{0,1:T(2,128)} %param.31) | copy-start | bytes 388
  35.6 54.7 %copy-start.3 = (bf16[256,256]{1,0:T(8,128)(2,1)S(1)}, bf16[256,256]{1,0:T(8,128)(2,1)}, u32[]{:S(2)}) copy-start(bf16[256,256]{1,0:T(8,128)(2,1)} %param.29) | copy-start | bytes 393220
  35.7 80.6 %copy-start.1 = (bf16[16,4096]{1,0:T(8,128)(2,1)S(1)}, bf16[16,4096]{1,0:T(8,128)(2,1)}, u32[]{:S(2)}) copy-start(bf16[16,4096]{1,0:T(8,128)(2,1)} %param.18) | copy-start | bytes 393220
  75.4 53.7 %copy-start.10 = (f32[16,2]{0,1:T(2,128)S(1)}, f32[16,2]{0,1:T(2,128)}, u32[]{:S(2)}) copy-start(f32[16,2]{0,1:T(2,128)} %param.32) | copy-start | bytes 388
  75.9 109.3 %copy-start.2 = (bf16[1,4096,128]{2,1,0:T(8,128)(2,1)S(1)}, bf16[1,4096,128]{2,1,0:T(8,128)(2,1)}, u32[]{:S(2)}) copy-start(bf16[1,4096,128]{2,1,0:T(8,128)(2,1)} %param.34) | copy-start | bytes 3145732
  79.9 10.3 %all-to-all-start.2 = ((bf16[16,16,256]{2,1,0:T(8,128)(2,1)}), bf16[16,16,256]{2,1,0:T(8,128)(2,1)S(1)}, u32[]{:S(2)}, u32[]{:S(2)}) async-start(bf16[16,16,256]{2,1,0:T(8,128)(2,1)} %broadcast_in_dim.22), calls=%async_computation.2 | async-start | bytes 262144 | tf_op jit(solution)/shard_map/all_to_all | solution.py:29
  91.1 11.0 %all-to-all-start.3 = ((bf16[16,16,256]{2,1,0:T(8,128)(2,1)}), bf16[16,16,256]{2,1,0:T(8,128)(2,1)}, u32[]{:S(2)}, u32[]{:S(2)}) async-start(bf16[16,16,256]{2,1,0:T(8,128)(2,1)} %bitcast.8), calls=%async_computation.3 | async-start | bytes 262144 | tf_op jit(solution)/shard_map/all_to_all | solution.py:119
  102.1 22.9 %all-to-all-start.4 = ((bf16[16,16,256]{2,1,0:T(8,128)(2,1)}), bf16[16,16,256]{2,1,0:T(8,128)(2,1)S(1)}, u32[]{:S(2)}, u32[]{:S(2)}) async-start(bf16[16,16,256]{2,1,0:T(8,128)(2,1)} %all-to-all-done.3), calls=%async_computation.4 | async-start | bytes 262144 | tf_op jit(solution)/shard_map/all_to_all | solution.py:17
  125.2 10.9 %copy-start.7 = (bf16[16,256]{1,0:T(8,128)(2,1)}, bf16[16,256]{1,0:T(8,128)(2,1)S(1)}, u32[]{:S(2)}) copy-start(bf16[16,256]{1,0:T(8,128)(2,1)S(1)} %get-tuple-element.6) | copy-start | bytes 24580
  125.8 10.2 %all-to-all-start.5 = ((f32[16,1,16]{2,1,0:T(1,128)}), f32[16,1,16]{2,1,0:T(1,128)S(1)}, u32[]{:S(2)}, u32[]{:S(2)}) async-start(f32[16,1,16]{2,1,0:T(1,128)} %broadcast_in_dim.23), calls=%async_computation.5 | async-start | bytes 16384 | tf_op jit(solution)/shard_map/all_to_all | solution.py:29
  145.5 3.3 %collective-permute-start = (bf16[64,256]{1,0:T(8,128)(2,1)S(1)}, bf16[64,256]{1,0:T(8,128)(2,1)S(1)}, u32[]{:S(2)}, u32[]{:S(2)}) collective-permute-start(bf16[64,256]{1,0:T(8,128)(2,1)S(1)} %all_to_all.65), channel_id=1, source_target_pairs={{0,1},{1,2},{2,3},{3,4},{4,5},{5,6},{6,7},{7,8},{8,9},{9,10},{10,1... | collective-permute-start | bytes 98312 | tf_op jit(solution)/shard_map/ppermute | solution.py:156
  148.8 4.1 %collective-permute-start.1 = (bf16[64,256]{1,0:T(8,128)(2,1)S(1)}, bf16[64,256]{1,0:T(8,128)(2,1)S(1)}, u32[]{:S(2)}, u32[]{:S(2)}) collective-permute-start(bf16[64,256]{1,0:T(8,128)(2,1)S(1)} %collective-permute-done), channel_id=1, source_target_pairs={{0,1},{1,2},{2,3},{3,4},{4,5},{5,6},{6,7},{7,8},{8,9},{9,10},{10,1... | collective-permute-start | bytes 98312 | tf_op jit(solution)/shard_map/ppermute | solution.py:156
  151.1 3.3 %collective-permute-start.8 = (bf16[64,256]{1,0:T(8,128)(2,1)S(1)}, bf16[64,256]{1,0:T(8,128)(2,1)S(1)}, u32[]{:S(2)}, u32[]{:S(2)}) collective-permute-start(bf16[64,256]{1,0:T(8,128)(2,1)S(1)} %all_to_all.65), channel_id=1, source_target_pairs={{0,15},{1,0},{2,1},{3,2},{4,3},{5,4},{6,5},{7,6},{8,7},{9,8},{10,9... | collective-permute-start | bytes 98312 | tf_op jit(solution)/shard_map/ppermute | solution.py:158
  152.9 4.6 %collective-permute-start.2 = (bf16[64,256]{1,0:T(8,128)(2,1)S(1)}, bf16[64,256]{1,0:T(8,128)(2,1)S(1)}, u32[]{:S(2)}, u32[]{:S(2)}) collective-permute-start(bf16[64,256]{1,0:T(8,128)(2,1)S(1)} %collective-permute-done.1), channel_id=1, source_target_pairs={{0,1},{1,2},{2,3},{3,4},{4,5},{5,6},{6,7},{7,8},{8,9},{9,10},{10,1... | collective-permute-start | bytes 98312 | tf_op jit(solution)/shard_map/ppermute | solution.py:156
  154.5 3.3 %collective-permute-start.9 = (bf16[64,256]{1,0:T(8,128)(2,1)S(1)}, bf16[64,256]{1,0:T(8,128)(2,1)S(1)}, u32[]{:S(2)}, u32[]{:S(2)}) collective-permute-start(bf16[64,256]{1,0:T(8,128)(2,1)S(1)} %collective-permute-done.8), channel_id=1, source_target_pairs={{0,15},{1,0},{2,1},{3,2},{4,3},{5,4},{6,5},{7,6},{8,7},{9,8},{10,9... | collective-permute-start | bytes 98312 | tf_op jit(solution)/shard_map/ppermute | solution.py:158
  157.4 4.6 %collective-permute-start.3 = (bf16[64,256]{1,0:T(8,128)(2,1)S(1)}, bf16[64,256]{1,0:T(8,128)(2,1)S(1)}, u32[]{:S(2)}, u32[]{:S(2)}) collective-permute-start(bf16[64,256]{1,0:T(8,128)(2,1)S(1)} %collective-permute-done.2), channel_id=1, source_target_pairs={{0,1},{1,2},{2,3},{3,4},{4,5},{5,6},{6,7},{7,8},{8,9},{9,10},{10,1... | collective-permute-start | bytes 98312 | tf_op jit(solution)/shard_map/ppermute | solution.py:156
  157.8 4.3 %collective-permute-start.10 = (bf16[64,256]{1,0:T(8,128)(2,1)S(1)}, bf16[64,256]{1,0:T(8,128)(2,1)S(1)}, u32[]{:S(2)}, u32[]{:S(2)}) collective-permute-start(bf16[64,256]{1,0:T(8,128)(2,1)S(1)} %collective-permute-done.9), channel_id=1, source_target_pairs={{0,15},{1,0},{2,1},{3,2},{4,3},{5,4},{6,5},{7,6},{8,7},{9,8},{10,9... | collective-permute-start | bytes 98312 | tf_op jit(solution)/shard_map/ppermute | solution.py:158
  162.0 4.6 %collective-permute-start.4 = (bf16[64,256]{1,0:T(8,128)(2,1)S(1)}, bf16[64,256]{1,0:T(8,128)(2,1)S(1)}, u32[]{:S(2)}, u32[]{:S(2)}) collective-permute-start(bf16[64,256]{1,0:T(8,128)(2,1)S(1)} %collective-permute-done.3), channel_id=1, source_target_pairs={{0,1},{1,2},{2,3},{3,4},{4,5},{5,6},{6,7},{7,8},{8,9},{9,10},{10,1... | collective-permute-start | bytes 98312 | tf_op jit(solution)/shard_map/ppermute | solution.py:156
  162.2 4.6 %collective-permute-start.11 = (bf16[64,256]{1,0:T(8,128)(2,1)S(1)}, bf16[64,256]{1,0:T(8,128)(2,1)S(1)}, u32[]{:S(2)}, u32[]{:S(2)}) collective-permute-start(bf16[64,256]{1,0:T(8,128)(2,1)S(1)} %collective-permute-done.10), channel_id=1, source_target_pairs={{0,15},{1,0},{2,1},{3,2},{4,3},{5,4},{6,5},{7,6},{8,7},{9,8},{10,9... | collective-permute-start | bytes 98312 | tf_op jit(solution)/shard_map/ppermute | solution.py:158
  166.5 4.6 %collective-permute-start.5 = (bf16[64,256]{1,0:T(8,128)(2,1)S(1)}, bf16[64,256]{1,0:T(8,128)(2,1)S(1)}, u32[]{:S(2)}, u32[]{:S(2)}) collective-permute-start(bf16[64,256]{1,0:T(8,128)(2,1)S(1)} %collective-permute-done.4), channel_id=1, source_target_pairs={{0,1},{1,2},{2,3},{3,4},{4,5},{5,6},{6,7},{7,8},{8,9},{9,10},{10,1... | collective-permute-start | bytes 98312 | tf_op jit(solution)/shard_map/ppermute | solution.py:156
  166.7 4.6 %collective-permute-start.12 = (bf16[64,256]{1,0:T(8,128)(2,1)S(1)}, bf16[64,256]{1,0:T(8,128)(2,1)S(1)}, u32[]{:S(2)}, u32[]{:S(2)}) collective-permute-start(bf16[64,256]{1,0:T(8,128)(2,1)S(1)} %collective-permute-done.11), channel_id=1, source_target_pairs={{0,15},{1,0},{2,1},{3,2},{4,3},{5,4},{6,5},{7,6},{8,7},{9,8},{10,9... | collective-permute-start | bytes 98312 | tf_op jit(solution)/shard_map/ppermute | solution.py:158
  171.1 4.6 %collective-permute-start.6 = (bf16[64,256]{1,0:T(8,128)(2,1)S(1)}, bf16[64,256]{1,0:T(8,128)(2,1)S(1)}, u32[]{:S(2)}, u32[]{:S(2)}) collective-permute-start(bf16[64,256]{1,0:T(8,128)(2,1)S(1)} %collective-permute-done.5), channel_id=1, source_target_pairs={{0,1},{1,2},{2,3},{3,4},{4,5},{5,6},{6,7},{7,8},{8,9},{9,10},{10,1... | collective-permute-start | bytes 98312 | tf_op jit(solution)/shard_map/ppermute | solution.py:156
  171.7 4.7 %collective-permute-start.13 = (bf16[64,256]{1,0:T(8,128)(2,1)S(1)}, bf16[64,256]{1,0:T(8,128)(2,1)S(1)}, u32[]{:S(2)}, u32[]{:S(2)}) collective-permute-start(bf16[64,256]{1,0:T(8,128)(2,1)S(1)} %collective-permute-done.12), channel_id=1, source_target_pairs={{0,15},{1,0},{2,1},{3,2},{4,3},{5,4},{6,5},{7,6},{8,7},{9,8},{10,9... | collective-permute-start | bytes 98312 | tf_op jit(solution)/shard_map/ppermute | solution.py:158
  175.6 4.7 %collective-permute-start.7 = (bf16[64,256]{1,0:T(8,128)(2,1)S(1)}, bf16[64,256]{1,0:T(8,128)(2,1)}, u32[]{:S(2)}, u32[]{:S(2)}) collective-permute-start(bf16[64,256]{1,0:T(8,128)(2,1)S(1)} %collective-permute-done.6), channel_id=1, source_target_pairs={{0,1},{1,2},{2,3},{3,4},{4,5},{5,6},{6,7},{7,8},{8,9},{9,10},{10,1... | collective-permute-start | bytes 98312 | tf_op jit(solution)/shard_map/ppermute | solution.py:156
  176.4 6.3 %collective-permute-start.14 = (bf16[64,256]{1,0:T(8,128)(2,1)S(1)}, bf16[64,256]{1,0:T(8,128)(2,1)S(1)}, u32[]{:S(2)}, u32[]{:S(2)}) collective-permute-start(bf16[64,256]{1,0:T(8,128)(2,1)S(1)} %collective-permute-done.13), channel_id=1, source_target_pairs={{0,15},{1,0},{2,1},{3,2},{4,3},{5,4},{6,5},{7,6},{8,7},{9,8},{10,9... | collective-permute-start | bytes 98312 | tf_op jit(solution)/shard_map/ppermute | solution.py:158
  185.1 31.9 %copy-start.11 = (f32[128]{0:T(128)S(1)}, f32[128]{0:T(128)}, u32[]{:S(2)}) copy-start(f32[128]{0:T(128)} %param.24) | copy-start | bytes 1540
  185.1 38.3 %copy-start.6 = (f32[16,64]{1,0:T(8,128)S(1)}, f32[16,64]{1,0:T(8,128)}, u32[]{:S(2)}) copy-start(f32[16,64]{1,0:T(8,128)} %get-tuple-element.4) | copy-start | bytes 12292
  185.1 38.3 %copy-start.8 = (bf16[16,256]{1,0:T(8,128)(2,1)S(1)}, bf16[16,256]{1,0:T(8,128)(2,1)}, u32[]{:S(2)}) copy-start(bf16[16,256]{1,0:T(8,128)(2,1)} %copy-done.7) | copy-start | bytes 24580
  188.3 24.5 %all-to-all-start.7 = ((bf16[16,64,256]{2,1,0:T(8,128)(2,1)}), bf16[16,64,256]{2,1,0:T(8,128)(2,1)S(1)}, u32[]{:S(2)}, u32[]{:S(2)}) async-start(bf16[16,64,256]{2,1,0:T(8,128)(2,1)} %bitcast.59), calls=%async_computation.7 | async-start | bytes 1048576 | tf_op jit(solution)/shard_map/all_to_all | solution.py:17
  213.4 9.9 %all-to-all-start.8 = ((bf16[16,4,256]{2,1,0:T(4,128)(2,1)}), bf16[16,4,256]{2,1,0:T(4,128)(2,1)S(1)}, u32[]{:S(2)}, u32[]{:S(2)}) async-start(bf16[16,4,256]{2,1,0:T(4,128)(2,1)} %all_to_all.67), calls=%async_computation.8 | async-start | bytes 65536 | tf_op jit(solution)/shard_map/all_to_all | solution.py:166
  (2 other events, 4.5 us)
